TPU v7x, 32 devices: a whole 2x2x4 slice. The times are simulated.
32 devices in a mesh: sp: 8 (over z, x), tp: 4 (over y, core).
Axes of the slice: x: 2, y: 2, z: 4, core: 2. Of those that a mesh axis runs over, the one named last changes fastest.
Arguments:
- queries: bfloat16 [4096, 1024], P('sp', 'tp'), may hold values from -5.5 to 5.5
- key_vectors: bfloat16 [4096, 1024], P('sp', 'tp'), may hold values from -5.5 to 5.5
- latents: bfloat16 [4096, 2048], P('sp', 'tp'), may hold values from -6 to 6
- w_value: bfloat16 [2048, 1024], P(None, 'tp'), may hold values from -0.125 to 0.125
- log_sums: float32 [4096, 16], P('sp', 'tp'), as said below
- out_pair: bfloat16 [4096, 2048], P('sp', 'tp'), may hold values from -6 to 6
- cotangent: bfloat16 [4096, 1024], P('sp', 'tp'), may hold values from -6 to 6
- lambdas: float32 [8], P('tp'), may hold values from 0.3 to 0.8
- out_gain: float32 [128], replicated, may hold values from 0.1 to 1.9
Outputs:
- query_grad: float32 [4096, 1024], P('sp', 'tp')
- key_grad: float32 [4096, 1024], P('sp', 'tp')
- value_grad: float32 [4096, 1024], P('sp', 'tp')
- weight_grad: float32 [2048, 1024], P('sp', 'tp')
Inputs may be any that keep to these rules, and one draw needn't show every extreme that they name: `log_sums`: each entry is the logarithm of the sum of exp(scores_c[t, s]) over s <= t for its row t, head h and map c.
All inputs are finite; a program needn't handle non-finite values.
Results may differ from a plain program's by a relative error of at most 0.008.
Values may be sent and summed in bfloat16 or wider, within the bound.
A program may use at most 64 MiB of HBM per device.

v0:
```python
import jax
import jax.numpy as jnp
from jax import lax
from jax.sharding import PartitionSpec as P

norm_floor = 0.25
block_rows = 512


def head_cotangent(out_pair, cotangent, lambdas, out_gain):
    tok_rows = out_pair.shape[0]
    head_count = lambdas.shape[0]
    out_maps = out_pair.astype(jnp.float32).reshape(tok_rows, head_count, 2, -1)
    lam_cols = lambdas[None, :, None]
    merged = out_maps[:, :, 0] - lam_cols * out_maps[:, :, 1]
    inv_norm = lax.rsqrt(jnp.mean(merged * merged, axis=-1, keepdims=True) + norm_floor)
    scaled = cotangent.astype(jnp.float32).reshape(merged.shape) * out_gain
    inner_dot = jnp.mean(scaled * merged, axis=-1, keepdims=True)
    out_grad = (inv_norm * scaled - merged * (inv_norm * inv_norm * inv_norm) * inner_dot).astype(
        jnp.bfloat16
    )
    grad_wide = out_grad.astype(jnp.float32)
    first_map = jnp.sum(grad_wide * out_maps[:, :, 0], axis=-1)
    second_map = -lambdas[None, :] * jnp.sum(grad_wide * out_maps[:, :, 1], axis=-1)
    return (out_grad, jnp.stack([first_map, second_map], axis=-1))


def block_terms(
    query_block,
    key_block,
    value_block,
    grad_block,
    log_block,
    term_block,
    lambdas,
    query_pos,
    key_pos,
):
    factor = query_block.shape[-1] ** (-0.5)
    scores = (
        jnp.einsum("qhcd,khcd->hcqk", query_block, key_block, preferred_element_type=jnp.float32)
        * factor
    )
    visible = key_pos[None, :] <= query_pos[:, None]
    shifted = scores - jnp.transpose(log_block, (1, 2, 0))[..., None]
    softmax_maps = jnp.where(visible, jnp.exp(shifted), 0.0)
    value_dot = jnp.einsum(
        "qhe,khe->hqk", grad_block, value_block, preferred_element_type=jnp.float32
    )
    lam_cols = lambdas[:, None, None]
    weights = (softmax_maps[:, 0] - lam_cols * softmax_maps[:, 1]).astype(jnp.bfloat16)
    term_cols = jnp.transpose(term_block, (1, 2, 0))
    first_map = softmax_maps[:, 0] * (value_dot - term_cols[:, 0, :, None])
    second_map = softmax_maps[:, 1] * (-lam_cols * value_dot - term_cols[:, 1, :, None])
    dscore = (jnp.stack([first_map, second_map], axis=1) * factor).astype(jnp.bfloat16)
    return (weights, dscore)


def block_span():
    return block_rows


def per_device(
    queries, key_vectors, latents, w_value, log_sums, out_pair, cotangent, lambdas, out_gain
):
    tok_rows = queries.shape[0]
    head_count = lambdas.shape[0]
    offset = lax.axis_index("sp") * tok_rows
    own_pos = offset + jnp.arange(tok_rows, dtype=jnp.int32)
    last_pos = offset + tok_rows - 1
    gathered = lax.all_gather(latents, "tp", axis=1, tiled=True)
    values = jnp.dot(gathered, w_value, preferred_element_type=jnp.float32).astype(jnp.bfloat16)
    out_grad, row_terms = head_cotangent(out_pair, cotangent, lambdas, out_gain)
    query_heads = queries.reshape(tok_rows, head_count, 2, -1)
    key_heads = key_vectors.reshape(tok_rows, head_count, 2, -1)
    value_heads = values.reshape(tok_rows, head_count, -1)
    log_heads = log_sums.reshape(tok_rows, head_count, 2)
    grad_flat = out_grad.reshape(tok_rows, -1)
    term_flat = row_terms.reshape(tok_rows, -1)
    zero_keys = jnp.zeros(key_heads.shape, jnp.float32)
    zero_values = jnp.zeros(value_heads.shape, jnp.float32)
    shards = (
        lax.all_gather(key_vectors, "sp", axis=0, tiled=True),
        lax.all_gather(values, "sp", axis=0, tiled=True),
    )
    key_piece = shards[0]
    value_piece = shards[1]
    piece_rows = key_piece.shape[0]
    block_len = block_span()

    def query_add_block(block_idx, partial_value):
        begin_row = block_idx * block_len
        key_block = lax.dynamic_slice_in_dim(key_piece, begin_row, block_len, 0).reshape(
            block_len, head_count, 2, -1
        )
        value_block = lax.dynamic_slice_in_dim(value_piece, begin_row, block_len, 0).reshape(
            block_len, head_count, -1
        )
        key_pos = begin_row + jnp.arange(block_len, dtype=jnp.int32)

        def query_compute(sums):
            weights, dscore = block_terms(
                query_heads,
                key_block,
                value_block,
                out_grad,
                log_heads,
                row_terms,
                lambdas,
                own_pos,
                key_pos,
            )
            return sums + jnp.einsum(
                "hcqk,khcd->qhcd", dscore, key_block, preferred_element_type=jnp.float32
            )

        return lax.cond(begin_row <= last_pos, query_compute, lambda sums: sums, partial_value)

    query_grad = lax.fori_loop(0, piece_rows // block_len, query_add_block, zero_keys)
    shards = (
        lax.all_gather(queries.astype(jnp.float32), "sp", axis=0, tiled=True).astype(jnp.bfloat16),
        lax.all_gather(grad_flat.astype(jnp.float32), "sp", axis=0, tiled=True).astype(
            jnp.bfloat16
        ),
        lax.all_gather(log_sums, "sp", axis=0, tiled=True),
        lax.all_gather(term_flat, "sp", axis=0, tiled=True),
    )
    query_piece = shards[0]
    grad_piece = shards[1]
    log_piece = shards[2]
    term_piece = shards[3]
    piece_rows = query_piece.shape[0]
    key_block_len = block_span()

    def key_add_block(block_idx, partial_value):
        begin_row = block_idx * key_block_len
        query_block = lax.dynamic_slice_in_dim(query_piece, begin_row, key_block_len, 0).reshape(
            key_block_len, head_count, 2, -1
        )
        grad_block = lax.dynamic_slice_in_dim(grad_piece, begin_row, key_block_len, 0).reshape(
            key_block_len, head_count, -1
        )
        log_block = lax.dynamic_slice_in_dim(log_piece, begin_row, key_block_len, 0).reshape(
            key_block_len, head_count, 2
        )
        term_block = lax.dynamic_slice_in_dim(term_piece, begin_row, key_block_len, 0).reshape(
            key_block_len, head_count, 2
        )
        query_pos = begin_row + jnp.arange(key_block_len, dtype=jnp.int32)

        def key_compute(sums):
            weights, dscore = block_terms(
                query_block,
                key_heads,
                value_heads,
                grad_block,
                log_block,
                term_block,
                lambdas,
                query_pos,
                own_pos,
            )
            key_sum = sums[0] + jnp.einsum(
                "hcqk,qhcd->khcd", dscore, query_block, preferred_element_type=jnp.float32
            )
            value_sum = sums[1] + jnp.einsum(
                "hqk,qhe->khe", weights, grad_block, preferred_element_type=jnp.float32
            )
            return (key_sum, value_sum)

        return lax.cond(
            begin_row + key_block_len - 1 >= offset, key_compute, lambda sums: sums, partial_value
        )

    key_grad, value_grad = lax.fori_loop(
        0, piece_rows // key_block_len, key_add_block, (zero_keys, zero_values)
    )
    value_flat = value_grad.reshape(tok_rows, -1)
    value_narrow = value_flat.astype(jnp.bfloat16)
    weight_grad = lax.psum_scatter(
        lax.dot_general(
            gathered, value_narrow, (((0,), (0,)), ((), ())), preferred_element_type=jnp.float32
        ),
        "sp",
        scatter_dimension=0,
        tiled=True,
    )
    return (
        query_grad.reshape(tok_rows, -1),
        key_grad.reshape(tok_rows, -1),
        value_flat,
        weight_grad,
    )


def solution(mesh):
    return jax.shard_map(
        per_device,
        mesh=mesh,
        in_specs=(
            P("sp", "tp"),
            P("sp", "tp"),
            P("sp", "tp"),
            P(None, "tp"),
            P("sp", "tp"),
            P("sp", "tp"),
            P("sp", "tp"),
            P("tp"),
            P(),
        ),
        out_specs=(P("sp", "tp"), P("sp", "tp"), P("sp", "tp"), P("sp", "tp")),
        check_vma=False,
    )
```

profile of v0, /device:TPU:0, one launch (start us, length us, event | category | flops | bytes accessed | tf_op | source)
XLA Modules:
  0.0 320.5 jit_solution(6820730226512585887)
XLA Ops:
  14.8 20.2 %all-gather.8.cloned.1.call-done = bf16[512,2048]{1,0:T(8,128)(2,1)} async-done(((bf16[512,512]{1,0:T(8,128)(2,1)}), bf16[512,2048]{1,0:T(8,128)(2,1)}) %all-gather.8.cloned.1.call-update) | async-done | bytes 2097168 | tf_op jit(solution)/shard_map/all_gather | solution.py:71
  34.9 3.1 convolution_convert_fusion
  38.7 31.0 %all_gather.25 = f32[4096,4]{0,1:T(4,128)S(1)} all-gather(f32[512,4]{0,1:T(4,128)S(1)} %copy-done.6), channel_id=1, replica_groups=mesh['sp'=8,'tp'=4] {'sp'}, dimensions={0}, use_global_device_ids=true | all-gather | bytes 73728 | tf_op jit(solution)/shard_map/all_gather | solution.py:125
  69.7 31.9 %all_gather.27 = f32[4096,4]{0,1:T(4,128)} all-gather(f32[512,4]{0,1:T(4,128)S(1)} %reshape.188), channel_id=1, replica_groups=mesh['sp'=8,'tp'=4] {'sp'}, dimensions={0}, use_global_device_ids=true | all-gather | bytes 73728 | tf_op jit(solution)/shard_map/all_gather | solution.py:126
  102.8 37.0 %all-gather.14.cloned.1.call-done = bf16[4096,256]{0,1:T(8,128)(2,1)} async-done(((bf16[512,256]{0,1:T(8,128)(2,1)}), bf16[4096,256]{0,1:T(8,128)(2,1)}) %all-gather.14.cloned.1.call-update) | async-done | bytes 2097168 | tf_op jit(solution)/shard_map/all_gather | solution.py:122
  139.9 90.7 %while.39 = (s32[]{:T(128)}, f32[512,2,2,64]{0,3,2,1:T(8,128)S(1)}, f32[512,2,128]{2,0,1:T(8,128)S(1)}, s32[]{:T(128)}, bf16[4096,256]{0,1:T(8,128)(2,1)}, /*ind...) while((s32[]{:T(128)}, f32[512,2,2,64]{0,3,2,1:T(8,128)S(1)}, ...), condition=%wide.region_11.12_spmd.clone.clone, body=%wide.region_8.11_spmd.clone.clone.sunk | while | flops 547881984 | bytes 43121072 | solution.py:175
  140.0 11.3 %conditional.8 = ((f32[512,2,2,64]{0,3,2,1:T(8,128)S(1)}, f32[512,2,128]{2,0,1:T(8,128)S(1)})) conditional(s32[]{:T(128)} %convert_element_type.110, (f32[512,2,2,64]{0,3,2,1:T(8,128)S(1)}, f32[512,2,128]{2,0,1:T(8,128)S(1)}) %tuple.152, (s32[]{:T(128)}, s32[]{:T(128)}, s32[512]{0:T(512)S(1)}, bf16[4096,256]{0,1:T(8,128)(2,1)}, ...), branch_computations={%region_9.9_spmd, %region_10.10_spmd} | conditional | flops 547881984 | bytes 43118728 | solution.py:171
  142.0 3.2 exponential_select_fusion
  145.2 2.9 multiply_bitcast_fusion.1
  151.3 11.3 %conditional.8 = ((f32[512,2,2,64]{0,3,2,1:T(8,128)S(1)}, f32[512,2,128]{2,0,1:T(8,128)S(1)})) conditional(s32[]{:T(128)} %convert_element_type.110, (f32[512,2,2,64]{0,3,2,1:T(8,128)S(1)}, f32[512,2,128]{2,0,1:T(8,128)S(1)}) %tuple.152, (s32[]{:T(128)}, s32[]{:T(128)}, s32[512]{0:T(512)S(1)}, bf16[4096,256]{0,1:T(8,128)(2,1)}, ...), branch_computations={%region_9.9_spmd, %region_10.10_spmd} | conditional | flops 547881984 | bytes 43118728 | solution.py:171
  153.4 3.2 exponential_select_fusion
  162.6 11.4 %conditional.8 = ((f32[512,2,2,64]{0,3,2,1:T(8,128)S(1)}, f32[512,2,128]{2,0,1:T(8,128)S(1)})) conditional(s32[]{:T(128)} %convert_element_type.110, (f32[512,2,2,64]{0,3,2,1:T(8,128)S(1)}, f32[512,2,128]{2,0,1:T(8,128)S(1)}) %tuple.152, (s32[]{:T(128)}, s32[]{:T(128)}, s32[512]{0:T(512)S(1)}, bf16[4096,256]{0,1:T(8,128)(2,1)}, ...), branch_computations={%region_9.9_spmd, %region_10.10_spmd} | conditional | flops 547881984 | bytes 43118728 | solution.py:171
  164.7 3.2 exponential_select_fusion
  167.9 3.1 multiply_bitcast_fusion.1
  174.1 11.3 %conditional.8 = ((f32[512,2,2,64]{0,3,2,1:T(8,128)S(1)}, f32[512,2,128]{2,0,1:T(8,128)S(1)})) conditional(s32[]{:T(128)} %convert_element_type.110, (f32[512,2,2,64]{0,3,2,1:T(8,128)S(1)}, f32[512,2,128]{2,0,1:T(8,128)S(1)}) %tuple.152, (s32[]{:T(128)}, s32[]{:T(128)}, s32[512]{0:T(512)S(1)}, bf16[4096,256]{0,1:T(8,128)(2,1)}, ...), branch_computations={%region_9.9_spmd, %region_10.10_spmd} | conditional | flops 547881984 | bytes 43118728 | solution.py:171
  176.1 3.2 exponential_select_fusion
  185.4 11.2 %conditional.8 = ((f32[512,2,2,64]{0,3,2,1:T(8,128)S(1)}, f32[512,2,128]{2,0,1:T(8,128)S(1)})) conditional(s32[]{:T(128)} %convert_element_type.110, (f32[512,2,2,64]{0,3,2,1:T(8,128)S(1)}, f32[512,2,128]{2,0,1:T(8,128)S(1)}) %tuple.152, (s32[]{:T(128)}, s32[]{:T(128)}, s32[512]{0:T(512)S(1)}, bf16[4096,256]{0,1:T(8,128)(2,1)}, ...), branch_computations={%region_9.9_spmd, %region_10.10_spmd} | conditional | flops 547881984 | bytes 43118728 | solution.py:171
  187.4 3.2 exponential_select_fusion
  196.7 11.3 %conditional.8 = ((f32[512,2,2,64]{0,3,2,1:T(8,128)S(1)}, f32[512,2,128]{2,0,1:T(8,128)S(1)})) conditional(s32[]{:T(128)} %convert_element_type.110, (f32[512,2,2,64]{0,3,2,1:T(8,128)S(1)}, f32[512,2,128]{2,0,1:T(8,128)S(1)}) %tuple.152, (s32[]{:T(128)}, s32[]{:T(128)}, s32[512]{0:T(512)S(1)}, bf16[4096,256]{0,1:T(8,128)(2,1)}, ...), branch_computations={%region_9.9_spmd, %region_10.10_spmd} | conditional | flops 547881984 | bytes 43118728 | solution.py:171
  198.7 3.2 exponential_select_fusion
  202.0 2.9 multiply_bitcast_fusion.1
  208.0 11.2 %conditional.8 = ((f32[512,2,2,64]{0,3,2,1:T(8,128)S(1)}, f32[512,2,128]{2,0,1:T(8,128)S(1)})) conditional(s32[]{:T(128)} %convert_element_type.110, (f32[512,2,2,64]{0,3,2,1:T(8,128)S(1)}, f32[512,2,128]{2,0,1:T(8,128)S(1)}) %tuple.152, (s32[]{:T(128)}, s32[]{:T(128)}, s32[512]{0:T(512)S(1)}, bf16[4096,256]{0,1:T(8,128)(2,1)}, ...), branch_computations={%region_9.9_spmd, %region_10.10_spmd} | conditional | flops 547881984 | bytes 43118728 | solution.py:171
  210.1 3.2 exponential_select_fusion
  213.3 2.9 multiply_bitcast_fusion.1
  219.3 11.3 %conditional.8 = ((f32[512,2,2,64]{0,3,2,1:T(8,128)S(1)}, f32[512,2,128]{2,0,1:T(8,128)S(1)})) conditional(s32[]{:T(128)} %convert_element_type.110, (f32[512,2,2,64]{0,3,2,1:T(8,128)S(1)}, f32[512,2,128]{2,0,1:T(8,128)S(1)}) %tuple.152, (s32[]{:T(128)}, s32[]{:T(128)}, s32[512]{0:T(512)S(1)}, bf16[4096,256]{0,1:T(8,128)(2,1)}, ...), branch_computations={%region_9.9_spmd, %region_10.10_spmd} | conditional | flops 547881984 | bytes 43118728 | solution.py:171
  221.4 3.2 exponential_select_fusion
  224.6 3.0 multiply_bitcast_fusion.1
  230.7 3.9 %convolution_bitcast_fusion.1 = f32[2048,256]{0,1:T(8,128)} fusion(bf16[512,2048]{1,0:T(8,128)(2,1)} %all-gather.8.cloned.1.call-done, f32[512,256]{1,0:T(8,128)S(1)} %copy_bitcast_fusion.2), kind=kOutput, calls=%fused_computation.46 | convolution fusion | flops 537001984 | bytes 4718592 | tf_op jit(solution)/shard_map/dot_general | solution.py:181
  235.8 5.5 %all-gather.10.cloned.1.call-done = bf16[4096,256]{0,1:T(8,128)(2,1)} async-done(((bf16[512,256]{0,1:T(8,128)(2,1)}), bf16[4096,256]{0,1:T(8,128)(2,1)}) %all-gather.10.cloned.1.call-update) | async-done | bytes 2097168 | tf_op jit(solution)/shard_map/all_gather | solution.py:84
  241.4 4.3 %while.38 = (s32[]{:T(128)}, f32[512,2,2,64]{0,3,2,1:T(8,128)S(1)}, s32[]{:T(128)}, bf16[4096,256]{0,1:T(8,128)(2,1)}, bf16[512,2,2,64]{0,3,2,1:T(8,128)(2,1)S(1...) while((s32[]{:T(128)}, f32[512,2,2,64]{0,3,2,1:T(8,128)S(1)}, ...), condition=%wide.region_7.8_spmd.clone, body=%wide.region_4.7_spmd.clone.sunk | while | flops 411960320 | bytes 20756812 | solution.py:119
  241.4 3.9 %conditional.7 = (f32[512,2,2,64]{0,3,2,1:T(8,128)S(1)}) conditional(s32[]{:T(128)} %convert_element_type.109, f32[512,2,2,64]{0,3,2,1:T(8,128)S(1)} %get-tuple-element.1245, (s32[]{:T(128)}, s32[512]{0:T(512)S(1)}, s32[]{:T(128)}, bf16[4096,256]{0,1:T(8,128)(2,1)}, bf16[512,2,2,64]{0,3,2,1:T(8,128)(2,1)S(1)}, /*index=5*/f32[512,2,2]{0,2,1:T(2,128)S(1)}, ...), branch_computations={%region_5.0_spmd, %region_6.6_spmd} | conditional | flops 411960320 | bytes 20754510 | solution.py:117
  246.7 65.2 %reduce-scatter.2.cloned.1.call-done = f32[256,256]{0,1:T(8,128)} async-done(((f32[2048,256]{0,1:T(8,128)}), f32[256,256]{0,1:T(8,128)}) %reduce-scatter.2.cloned.1.call-update) | async-done | bytes 262160 | tf_op jit(solution)/shard_map/reduce_scatter | solution.py:180
  (202 shorter events, 66.7 us)
Async XLA Ops:
  7.2 27.7 %copy-start = (bf16[2048,256]{1,0:T(8,128)(2,1)S(1)}, bf16[2048,256]{1,0:T(8,128)(2,1)}, u32[]{:S(2)}) copy-start(bf16[2048,256]{1,0:T(8,128)(2,1)} %param.20) | copy-start | bytes 3145732
  7.2 3.9 %copy-start.5 = (bf16[512,256]{1,0:T(8,128)(2,1)S(1)}, bf16[512,256]{1,0:T(8,128)(2,1)}, u32[]{:S(2)}) copy-start(bf16[512,256]{1,0:T(8,128)(2,1)} %param.23) | copy-start | bytes 786436
  7.2 4.1 %copy-start.8 = (f32[128]{0:T(128)S(1)}, f32[128]{0:T(128)}, u32[]{:S(2)}) copy-start(f32[128]{0:T(128)} %param.25) | copy-start | bytes 1540
  7.2 4.1 %copy-start.7 = (f32[2]{0:T(128)S(1)}, f32[2]{0:T(128)}, u32[]{:S(2)}) copy-start(f32[2]{0:T(128)} %param.24) | copy-start | bytes 28
  7.2 27.7 %all-gather.8.cloned.1.call-start = ((), (), s32[]{:S(2)}) async-start(), calls=%async_computation.2 | async-start | bytes 2621440 | tf_op jit(solution)/shard_map/all_gather | solution.py:71
  7.9 94.8 %all-gather.12.cloned.1.call-start = ((), (), s32[]{:S(2)}) async-start(), calls=%async_computation.4 | async-start | bytes 2359296 | tf_op jit(solution)/shard_map/all_gather | solution.py:121
  9.8 130.0 %all-gather.14.cloned.1.call-start = ((), (), s32[]{:S(2)}) async-start(), calls=%async_computation.5 | async-start | bytes 2359296 | tf_op jit(solution)/shard_map/all_gather | solution.py:122
  12.8 222.9 %all-gather.6.cloned.1.call-start = ((), (), s32[]{:S(2)}) async-start(), calls=%async_computation.1 | async-start | bytes 2359296 | tf_op jit(solution)/shard_map/all_gather | solution.py:83
  14.7 226.6 %all-gather.10.cloned.1.call-start = ((), (), s32[]{:S(2)}) async-start(), calls=%async_computation.3 | async-start | bytes 2359296 | tf_op jit(solution)/shard_map/all_gather | solution.py:84
  38.0 0.7 copy-start.6
  38.0 101.9 %copy-start.4 = (bf16[512,256]{0,1:T(8,128)(2,1)S(1)}, bf16[512,256]{0,1:T(8,128)(2,1)}, u32[]{:S(2)}) copy-start(bf16[512,256]{0,1:T(8,128)(2,1)} %copy.47) | copy-start | bytes 786436
  38.0 273.8 %reduce-scatter.2.cloned.1.call-start = ((), (), s32[]{:S(2)}) async-start(), calls=%async_computation.6 | async-start | bytes 2359296 | tf_op jit(solution)/shard_map/reduce_scatter | solution.py:180
  148.2 2.3 copy-start.1
  159.6 2.2 copy-start.1
  171.0 2.2 copy-start.1
  182.3 2.2 copy-start.1
  193.6 2.2 copy-start.1
  204.9 2.2 copy-start.1
  216.2 2.2 copy-start.1
  227.6 2.2 copy-start.1
  230.7 3.9 %copy-start.2 = (f32[512,256]{1,0:T(8,128)}, f32[512,256]{1,0:T(8,128)S(1)}, u32[]{:S(2)}) copy-start(f32[512,256]{1,0:T(8,128)S(1)} %copy_bitcast_fusion.2) | copy-start | bytes 1572868
  234.6 6.8 %copy-start.3 = (bf16[512,256]{0,1:T(8,128)(2,1)S(1)}, bf16[512,256]{0,1:T(8,128)(2,1)}, u32[]{:S(2)}) copy-start(bf16[512,256]{0,1:T(8,128)(2,1)} %copy.48) | copy-start | bytes 786436
Sparse Core Ops, SparseCore 0:
  9.6 25.2 all-gather.7
  37.5 50.9 all-gather.11
  91.1 48.6 all-gather.13
  142.3 48.5 all-gather.5
  192.7 48.5 all-gather.9
  244.7 67.0 reduce-scatter.1
where the time goes:
time: 322 us; the launch traced here: 320 us
  waiting for transfers between devices  129 us (40%)
  matrix products  69.3 us (22%)
  blocking collectives  62.9 us (20%)
  local copies, waits for them, and re-layouts  39.8 us (12%)
  between operations  14.3 us (4%)
  other arithmetic  3.63 us (1%)
    reduce_scatter x1, waiting for transfers between devices, per_device(): lax.psum_scatter(lax.dot_general(gathered, value_narrow, (((0,), (0,)), (...  65.2 us
    all_gather x1, waiting for transfers between devices, per_device(): lax.all_gather(grad_flat.astype(jnp.float32), 'sp', axis=0, tiled=True)  37 us
    all_gather x1, blocking collectives, per_device(): lax.all_gather(term_flat, 'sp', axis=0, tiled=True)  31.9 us
    all_gather x1, blocking collectives, per_device(): lax.all_gather(log_sums, 'sp', axis=0, tiled=True)  31 us
    dot_general x9, matrix products, block_terms(): jnp.einsum('qhcd,khcd->hcqk', query_block, key_block, preferred_element_t...  26.6 us
    dot_general x9, matrix products, block_terms(): jnp.einsum('qhe,khe->hqk', grad_block, value_block, preferred_element_typ...  24.4 us
    all_gather x1, waiting for transfers between devices, per_device(): gathered = lax.all_gather(latents, 'tp', axis=1, tiled=True)  20.2 us
    cond x32, local copies, waits for them, and re-layouts  13.3 us
  transfers between devices with their start and end apart: 6, of which 4 were waited for; matrix products, arithmetic and copies ran while one was open for 30% of the time, Pallas kernels for 0%

commit v1 on v0

--- a/solution.py
+++ b/solution.py
@@ -68,7 +68,9 @@
     offset = lax.axis_index("sp") * tok_rows
     own_pos = offset + jnp.arange(tok_rows, dtype=jnp.int32)
     last_pos = offset + tok_rows - 1
-    gathered = lax.all_gather(latents, "tp", axis=1, tiled=True)
+    gathered = jnp.concatenate(
+        lax.all_to_all(jnp.stack([latents] * lax.axis_size("tp")), "tp", 0, 0), axis=1
+    )
     values = jnp.dot(gathered, w_value, preferred_element_type=jnp.float32).astype(jnp.bfloat16)
     out_grad, row_terms = head_cotangent(out_pair, cotangent, lambdas, out_gain)
     query_heads = queries.reshape(tok_rows, head_count, 2, -1)

time: 322 us -> 297 us (0.922)
  waiting for transfers between devices: 129 us -> 77.4 us
  blocking collectives: 62.9 us -> 91.8 us
    all_gather x1, waiting for transfers between devices: 37 us -> 2.82 us  [per_device(): lax.all_gather(grad_flat.astype(jnp.float32), 'sp', axis=0, tiled=True)]
    all_to_all x0 -> x1, blocking collectives: none -> 29.7 us  [per_device(): lax.all_to_all(jnp.stack([latents] * lax.axis_size('tp')), 'tp', 0, 0)]
    all_gather x1 -> x0, waiting for transfers between devices: 20.2 us -> none  [per_device(): gathered = lax.all_gather(latents, 'tp', axis=1, tiled=True)]
    dynamic_slice x8, local copies, waits for them, and re-layouts: 5.66 us -> 0.09 us  [key_add_block(): lax.dynamic_slice_in_dim(term_piece, begin_row, key_block_len, 0)]
    all_gather x1, waiting for transfers between devices: 5.54 us -> 9.21 us  [per_device(): lax.all_gather(values, 'sp', axis=0, tiled=True)]
    unnamed x25 -> x30, local copies, waits for them, and re-layouts: 10.3 us -> 13.7 us
    cond x32 -> x48, local copies, waits for them, and re-layouts: 13.3 us -> 13.4 us
  transfers between devices with their start and end apart: 6 -> 5, of which waited for: 4 -> 3; matrix products, arithmetic and copies ran while one was open for 30% -> 31% of each run, Pallas kernels for 0% -> 0%
where the time goes in v1:
time: 297 us; the launch traced here: 296 us
  blocking collectives  91.8 us (31%)
  waiting for transfers between devices  77.4 us (26%)
  matrix products  67.7 us (23%)
  local copies, waits for them, and re-layouts  38.7 us (13%)
  between operations  14 us (5%)
  other arithmetic  4.34 us (1%)
    reduce_scatter x1, waiting for transfers between devices, per_device(): lax.psum_scatter(lax.dot_general(gathered, value_narrow, (((0,), (0,)), (...  65.2 us
    all_gather x1, blocking collectives, per_device(): lax.all_gather(log_sums, 'sp', axis=0, tiled=True)  31.2 us
    all_gather x1, blocking collectives, per_device(): lax.all_gather(term_flat, 'sp', axis=0, tiled=True)  30.9 us
    all_to_all x1, blocking collectives, per_device(): lax.all_to_all(jnp.stack([latents] * lax.axis_size('tp')), 'tp', 0, 0)  29.7 us
    dot_general x9, matrix products, block_terms(): jnp.einsum('qhcd,khcd->hcqk', query_block, key_block, preferred_element_t...  26.7 us
    dot_general x9, matrix products, block_terms(): jnp.einsum('qhe,khe->hqk', grad_block, value_block, preferred_element_typ...  24.5 us
    unnamed x30, local copies, waits for them, and re-layouts  13.7 us
    cond x48, local copies, waits for them, and re-layouts  13.4 us
  transfers between devices with their start and end apart: 5, of which 3 were waited for; matrix products, arithmetic and copies ran while one was open for 31% of the time, Pallas kernels for 0%

profile of v1, /device:TPU:0, one launch (start us, length us, event | category | flops | bytes accessed | tf_op | source)
XLA Modules:
  0.0 296.0 jit_solution(5063968905553990007)
XLA Ops:
  16.5 29.7 %all_to_all.5 = bf16[4,512,512]{1,2,0:T(8,128)(2,1)S(1)} all-to-all(bf16[4,512,512]{1,2,0:T(8,128)(2,1)S(1)} %stack.50), channel_id=1, replica_groups=mesh['sp'=8,'tp'=4] {'tp'}, dimensions={0} | all-to-all | bytes 4194304 | tf_op jit(solution)/shard_map/all_to_all | solution.py:72
  50.2 31.2 %all_gather.21 = f32[4096,4]{0,1:T(4,128)S(1)} all-gather(f32[512,4]{0,1:T(4,128)S(1)} %copy-done.7), channel_id=1, replica_groups=mesh['sp'=8,'tp'=4] {'sp'}, dimensions={0}, use_global_device_ids=true | all-gather | bytes 73728 | tf_op jit(solution)/shard_map/all_gather | solution.py:127
  81.4 30.9 %all_gather.23 = f32[4096,4]{0,1:T(4,128)S(1)} all-gather(f32[512,4]{0,1:T(4,128)S(1)} %reshape.199), channel_id=1, replica_groups=mesh['sp'=8,'tp'=4] {'sp'}, dimensions={0}, use_global_device_ids=true | all-gather | bytes 73728 | tf_op jit(solution)/shard_map/all_gather | solution.py:128
  115.4 85.6 %while.39 = (s32[]{:T(128)}, f32[512,2,2,64]{0,3,2,1:T(8,128)S(1)}, f32[512,2,128]{2,0,1:T(8,128)S(1)}, s32[]{:T(128)}, bf16[4096,256]{0,1:T(8,128)(2,1)}, /*ind...) while((s32[]{:T(128)}, f32[512,2,2,64]{0,3,2,1:T(8,128)S(1)}, ...), condition=%wide.region_11.12_spmd.clone.clone, body=%wide.region_8.11_spmd.clone.clone.sunk | while | flops 547881984 | bytes 43121128 | solution.py:177
  115.5 10.7 %conditional.8 = ((f32[512,2,2,64]{0,3,2,1:T(8,128)S(1)}, f32[512,2,128]{2,0,1:T(8,128)S(1)})) conditional(s32[]{:T(128)} %convert_element_type.112, (f32[512,2,2,64]{0,3,2,1:T(8,128)S(1)}, f32[512,2,128]{2,0,1:T(8,128)S(1)}) %tuple.152, (s32[]{:T(128)}, s32[]{:T(128)}, s32[512]{0:T(512)S(1)}, bf16[4096,256]{0,1:T(8,128)(2,1)}, ...), branch_computations={%region_9.9_spmd, %region_10.10_spmd} | conditional | flops 547881984 | bytes 43118784 | solution.py:173
  116.9 3.2 %exponential_select_fusion = f32[2,2,512,512]{3,2,1,0:T(8,128)} fusion(bf16[512,2,2,64]{0,3,2,1:T(8,128)(2,1)S(1)} %bitcast.178, bf16[512,2,2,64]{0,3,2,1:T(8,128)(2,1)S(1)} %get-tuple-element.842, f32[2,2,512]{2,1,0:T(2,128)S(1)} %bitcast.192, pred[512,512]{1,0:T(8,128)(4,1)S(1)} %broadcast_compare_fusion.1), kind=kOutput, calls=%fused_computation.24 | convolution fusion | flops 137363456 | bytes 4988928 | tf_op jit(solution)/shard_map/while/body/eval_jaxpr/cond/branch_1_fun/qhcd,khcd->hcqk/dot_general | solution.py:41
  120.1 2.9 multiply_bitcast_fusion.1
  126.2 10.6 %conditional.8 = ((f32[512,2,2,64]{0,3,2,1:T(8,128)S(1)}, f32[512,2,128]{2,0,1:T(8,128)S(1)})) conditional(s32[]{:T(128)} %convert_element_type.112, (f32[512,2,2,64]{0,3,2,1:T(8,128)S(1)}, f32[512,2,128]{2,0,1:T(8,128)S(1)}) %tuple.152, (s32[]{:T(128)}, s32[]{:T(128)}, s32[512]{0:T(512)S(1)}, bf16[4096,256]{0,1:T(8,128)(2,1)}, ...), branch_computations={%region_9.9_spmd, %region_10.10_spmd} | conditional | flops 547881984 | bytes 43118784 | solution.py:173
  127.6 3.2 %exponential_select_fusion = f32[2,2,512,512]{3,2,1,0:T(8,128)} fusion(bf16[512,2,2,64]{0,3,2,1:T(8,128)(2,1)S(1)} %bitcast.178, bf16[512,2,2,64]{0,3,2,1:T(8,128)(2,1)S(1)} %get-tuple-element.842, f32[2,2,512]{2,1,0:T(2,128)S(1)} %bitcast.192, pred[512,512]{1,0:T(8,128)(4,1)S(1)} %broadcast_compare_fusion.1), kind=kOutput, calls=%fused_computation.24 | convolution fusion | flops 137363456 | bytes 4988928 | tf_op jit(solution)/shard_map/while/body/eval_jaxpr/cond/branch_1_fun/qhcd,khcd->hcqk/dot_general | solution.py:41
  130.9 3.0 multiply_bitcast_fusion.1
  136.9 10.7 %conditional.8 = ((f32[512,2,2,64]{0,3,2,1:T(8,128)S(1)}, f32[512,2,128]{2,0,1:T(8,128)S(1)})) conditional(s32[]{:T(128)} %convert_element_type.112, (f32[512,2,2,64]{0,3,2,1:T(8,128)S(1)}, f32[512,2,128]{2,0,1:T(8,128)S(1)}) %tuple.152, (s32[]{:T(128)}, s32[]{:T(128)}, s32[512]{0:T(512)S(1)}, bf16[4096,256]{0,1:T(8,128)(2,1)}, ...), branch_computations={%region_9.9_spmd, %region_10.10_spmd} | conditional | flops 547881984 | bytes 43118784 | solution.py:173
  138.3 3.2 %exponential_select_fusion = f32[2,2,512,512]{3,2,1,0:T(8,128)} fusion(bf16[512,2,2,64]{0,3,2,1:T(8,128)(2,1)S(1)} %bitcast.178, bf16[512,2,2,64]{0,3,2,1:T(8,128)(2,1)S(1)} %get-tuple-element.842, f32[2,2,512]{2,1,0:T(2,128)S(1)} %bitcast.192, pred[512,512]{1,0:T(8,128)(4,1)S(1)} %broadcast_compare_fusion.1), kind=kOutput, calls=%fused_computation.24 | convolution fusion | flops 137363456 | bytes 4988928 | tf_op jit(solution)/shard_map/while/body/eval_jaxpr/cond/branch_1_fun/qhcd,khcd->hcqk/dot_general | solution.py:41
  141.5 2.9 multiply_bitcast_fusion.1
  147.6 10.6 %conditional.8 = ((f32[512,2,2,64]{0,3,2,1:T(8,128)S(1)}, f32[512,2,128]{2,0,1:T(8,128)S(1)})) conditional(s32[]{:T(128)} %convert_element_type.112, (f32[512,2,2,64]{0,3,2,1:T(8,128)S(1)}, f32[512,2,128]{2,0,1:T(8,128)S(1)}) %tuple.152, (s32[]{:T(128)}, s32[]{:T(128)}, s32[512]{0:T(512)S(1)}, bf16[4096,256]{0,1:T(8,128)(2,1)}, ...), branch_computations={%region_9.9_spmd, %region_10.10_spmd} | conditional | flops 547881984 | bytes 43118784 | solution.py:173
  149.0 3.2 %exponential_select_fusion = f32[2,2,512,512]{3,2,1,0:T(8,128)} fusion(bf16[512,2,2,64]{0,3,2,1:T(8,128)(2,1)S(1)} %bitcast.178, bf16[512,2,2,64]{0,3,2,1:T(8,128)(2,1)S(1)} %get-tuple-element.842, f32[2,2,512]{2,1,0:T(2,128)S(1)} %bitcast.192, pred[512,512]{1,0:T(8,128)(4,1)S(1)} %broadcast_compare_fusion.1), kind=kOutput, calls=%fused_computation.24 | convolution fusion | flops 137363456 | bytes 4988928 | tf_op jit(solution)/shard_map/while/body/eval_jaxpr/cond/branch_1_fun/qhcd,khcd->hcqk/dot_general | solution.py:41
  152.3 3.0 multiply_bitcast_fusion.1
  158.3 10.6 %conditional.8 = ((f32[512,2,2,64]{0,3,2,1:T(8,128)S(1)}, f32[512,2,128]{2,0,1:T(8,128)S(1)})) conditional(s32[]{:T(128)} %convert_element_type.112, (f32[512,2,2,64]{0,3,2,1:T(8,128)S(1)}, f32[512,2,128]{2,0,1:T(8,128)S(1)}) %tuple.152, (s32[]{:T(128)}, s32[]{:T(128)}, s32[512]{0:T(512)S(1)}, bf16[4096,256]{0,1:T(8,128)(2,1)}, ...), branch_computations={%region_9.9_spmd, %region_10.10_spmd} | conditional | flops 547881984 | bytes 43118784 | solution.py:173
  159.7 3.2 %exponential_select_fusion = f32[2,2,512,512]{3,2,1,0:T(8,128)} fusion(bf16[512,2,2,64]{0,3,2,1:T(8,128)(2,1)S(1)} %bitcast.178, bf16[512,2,2,64]{0,3,2,1:T(8,128)(2,1)S(1)} %get-tuple-element.842, f32[2,2,512]{2,1,0:T(2,128)S(1)} %bitcast.192, pred[512,512]{1,0:T(8,128)(4,1)S(1)} %broadcast_compare_fusion.1), kind=kOutput, calls=%fused_computation.24 | convolution fusion | flops 137363456 | bytes 4988928 | tf_op jit(solution)/shard_map/while/body/eval_jaxpr/cond/branch_1_fun/qhcd,khcd->hcqk/dot_general | solution.py:41
  168.9 10.7 %conditional.8 = ((f32[512,2,2,64]{0,3,2,1:T(8,128)S(1)}, f32[512,2,128]{2,0,1:T(8,128)S(1)})) conditional(s32[]{:T(128)} %convert_element_type.112, (f32[512,2,2,64]{0,3,2,1:T(8,128)S(1)}, f32[512,2,128]{2,0,1:T(8,128)S(1)}) %tuple.152, (s32[]{:T(128)}, s32[]{:T(128)}, s32[512]{0:T(512)S(1)}, bf16[4096,256]{0,1:T(8,128)(2,1)}, ...), branch_computations={%region_9.9_spmd, %region_10.10_spmd} | conditional | flops 547881984 | bytes 43118784 | solution.py:173
  170.3 3.2 %exponential_select_fusion = f32[2,2,512,512]{3,2,1,0:T(8,128)} fusion(bf16[512,2,2,64]{0,3,2,1:T(8,128)(2,1)S(1)} %bitcast.178, bf16[512,2,2,64]{0,3,2,1:T(8,128)(2,1)S(1)} %get-tuple-element.842, f32[2,2,512]{2,1,0:T(2,128)S(1)} %bitcast.192, pred[512,512]{1,0:T(8,128)(4,1)S(1)} %broadcast_compare_fusion.1), kind=kOutput, calls=%fused_computation.24 | convolution fusion | flops 137363456 | bytes 4988928 | tf_op jit(solution)/shard_map/while/body/eval_jaxpr/cond/branch_1_fun/qhcd,khcd->hcqk/dot_general | solution.py:41
  173.5 3.1 %multiply_bitcast_fusion.1 = (f32[2,1,512,512]{3,2,0,1:T(8,128)S(1)}, f32[2,1,512,512]{3,2,0,1:T(8,128)S(1)}) fusion(f32[2,2,512,512]{3,2,1,0:T(8,128)} %exponential_select_fusion, f32[2,512]{1,0:T(2,128)S(1)} %bitcast.189, f32[2,512]{1,0:T(2,128)S(1)} %bitcast.190, f32[2]{0:T(128)S(1)} %neg.16, bf16[512,2,128]{0,2,1:T(8,128)(2,1)S(1)} %bitcast.172, ...), kind=kOutput, calls=%fused_computation.31 | convolution fusion | flops 136839168 | bytes 8921096 | tf_op jit(solution)/shard_map/while/body/eval_jaxpr/cond/branch_1_fun/qhe,khe->hqk/dot_general | solution.py:47
  179.7 10.6 %conditional.8 = ((f32[512,2,2,64]{0,3,2,1:T(8,128)S(1)}, f32[512,2,128]{2,0,1:T(8,128)S(1)})) conditional(s32[]{:T(128)} %convert_element_type.112, (f32[512,2,2,64]{0,3,2,1:T(8,128)S(1)}, f32[512,2,128]{2,0,1:T(8,128)S(1)}) %tuple.152, (s32[]{:T(128)}, s32[]{:T(128)}, s32[512]{0:T(512)S(1)}, bf16[4096,256]{0,1:T(8,128)(2,1)}, ...), branch_computations={%region_9.9_spmd, %region_10.10_spmd} | conditional | flops 547881984 | bytes 43118784 | solution.py:173
  181.1 3.2 %exponential_select_fusion = f32[2,2,512,512]{3,2,1,0:T(8,128)} fusion(bf16[512,2,2,64]{0,3,2,1:T(8,128)(2,1)S(1)} %bitcast.178, bf16[512,2,2,64]{0,3,2,1:T(8,128)(2,1)S(1)} %get-tuple-element.842, f32[2,2,512]{2,1,0:T(2,128)S(1)} %bitcast.192, pred[512,512]{1,0:T(8,128)(4,1)S(1)} %broadcast_compare_fusion.1), kind=kOutput, calls=%fused_computation.24 | convolution fusion | flops 137363456 | bytes 4988928 | tf_op jit(solution)/shard_map/while/body/eval_jaxpr/cond/branch_1_fun/qhcd,khcd->hcqk/dot_general | solution.py:41
  184.3 2.9 multiply_bitcast_fusion.1
  190.3 10.7 %conditional.8 = ((f32[512,2,2,64]{0,3,2,1:T(8,128)S(1)}, f32[512,2,128]{2,0,1:T(8,128)S(1)})) conditional(s32[]{:T(128)} %convert_element_type.112, (f32[512,2,2,64]{0,3,2,1:T(8,128)S(1)}, f32[512,2,128]{2,0,1:T(8,128)S(1)}) %tuple.152, (s32[]{:T(128)}, s32[]{:T(128)}, s32[512]{0:T(512)S(1)}, bf16[4096,256]{0,1:T(8,128)(2,1)}, ...), branch_computations={%region_9.9_spmd, %region_10.10_spmd} | conditional | flops 547881984 | bytes 43118784 | solution.py:173
  191.7 3.2 %exponential_select_fusion = f32[2,2,512,512]{3,2,1,0:T(8,128)} fusion(bf16[512,2,2,64]{0,3,2,1:T(8,128)(2,1)S(1)} %bitcast.178, bf16[512,2,2,64]{0,3,2,1:T(8,128)(2,1)S(1)} %get-tuple-element.842, f32[2,2,512]{2,1,0:T(2,128)S(1)} %bitcast.192, pred[512,512]{1,0:T(8,128)(4,1)S(1)} %broadcast_compare_fusion.1), kind=kOutput, calls=%fused_computation.24 | convolution fusion | flops 137363456 | bytes 4988928 | tf_op jit(solution)/shard_map/while/body/eval_jaxpr/cond/branch_1_fun/qhcd,khcd->hcqk/dot_general | solution.py:41
  195.0 3.0 %multiply_bitcast_fusion.1 = (f32[2,1,512,512]{3,2,0,1:T(8,128)S(1)}, f32[2,1,512,512]{3,2,0,1:T(8,128)S(1)}) fusion(f32[2,2,512,512]{3,2,1,0:T(8,128)} %exponential_select_fusion, f32[2,512]{1,0:T(2,128)S(1)} %bitcast.189, f32[2,512]{1,0:T(2,128)S(1)} %bitcast.190, f32[2]{0:T(128)S(1)} %neg.16, bf16[512,2,128]{0,2,1:T(8,128)(2,1)S(1)} %bitcast.172, ...), kind=kOutput, calls=%fused_computation.31 | convolution fusion | flops 136839168 | bytes 8921096 | tf_op jit(solution)/shard_map/while/body/eval_jaxpr/cond/branch_1_fun/qhe,khe->hqk/dot_general | solution.py:47
  201.2 3.7 %convolution_bitcast_fusion.1 = f32[2048,256]{0,1:T(8,128)} fusion(bf16[512,256]{0,1:T(8,128)(2,1)S(1)} %bitcast.184, bf16[512,2048]{0,1:T(8,128)(2,1)} %bitcast.177), kind=kOutput, calls=%fused_computation.46 | convolution fusion | flops 536870912 | bytes 4456448 | tf_op jit(solution)/shard_map/dot_general | solution.py:183
  207.8 9.2 %all-gather.7.cloned.1.call-done = bf16[4096,256]{0,1:T(8,128)(2,1)} async-done(((bf16[512,256]{0,1:T(8,128)(2,1)}), bf16[4096,256]{0,1:T(8,128)(2,1)}) %all-gather.7.cloned.1.call-update) | async-done | bytes 2097168 | tf_op jit(solution)/shard_map/all_gather | solution.py:86
  217.1 4.3 %while.38 = (s32[]{:T(128)}, f32[512,2,2,64]{0,3,2,1:T(8,128)S(1)}, s32[]{:T(128)}, bf16[4096,256]{0,1:T(8,128)(2,1)}, bf16[512,2,2,64]{0,3,2,1:T(8,128)(2,1)S(1...) while((s32[]{:T(128)}, f32[512,2,2,64]{0,3,2,1:T(8,128)S(1)}, ...), condition=%wide.region_7.8_spmd.clone, body=%wide.region_4.7_spmd.clone.sunk | while | flops 411960320 | bytes 20756812 | solution.py:121
  217.2 3.9 %conditional.7 = (f32[512,2,2,64]{0,3,2,1:T(8,128)S(1)}) conditional(s32[]{:T(128)} %convert_element_type.111, f32[512,2,2,64]{0,3,2,1:T(8,128)S(1)} %get-tuple-element.1245, (s32[]{:T(128)}, s32[512]{0:T(512)S(1)}, s32[]{:T(128)}, bf16[4096,256]{0,1:T(8,128)(2,1)}, bf16[512,2,2,64]{0,3,2,1:T(8,128)(2,1)S(1)}, /*index=5*/f32[512,2,2]{0,2,1:T(2,128)S(1)}, ...), branch_computations={%region_5.0_spmd, %region_6.6_spmd} | conditional | flops 411960320 | bytes 20754510 | solution.py:119
  222.4 65.2 %reduce-scatter.2.cloned.1.call-done = f32[256,256]{0,1:T(8,128)} async-done(((f32[2048,256]{0,1:T(8,128)}), f32[256,256]{0,1:T(8,128)}) %reduce-scatter.2.cloned.1.call-update) | async-done | bytes 262160 | tf_op jit(solution)/shard_map/reduce_scatter | solution.py:182
  (223 shorter events, 64.1 us)
Async XLA Ops:
  7.2 40.4 %copy-start = (bf16[2048,256]{1,0:T(8,128)(2,1)S(1)}, bf16[2048,256]{1,0:T(8,128)(2,1)}, u32[]{:S(2)}) copy-start(bf16[2048,256]{1,0:T(8,128)(2,1)} %param.20) | copy-start | bytes 3145732
  7.2 4.4 %copy-start.11 = (f32[128]{0:T(128)S(1)}, f32[128]{0:T(128)}, u32[]{:S(2)}) copy-start(f32[128]{0:T(128)} %param.25) | copy-start | bytes 1540
  7.2 4.4 %copy-start.8 = (f32[2]{0:T(128)S(1)}, f32[2]{0:T(128)}, u32[]{:S(2)}) copy-start(f32[2]{0:T(128)} %param.24) | copy-start | bytes 28
  7.2 105.3 %all-gather.9.cloned.1.call-start = ((), (), s32[]{:S(2)}) async-start(), calls=%async_computation.4 | async-start | bytes 2359296 | tf_op jit(solution)/shard_map/all_gather | solution.py:123
  9.1 106.2 %all-gather.11.cloned.1.call-start = ((), (), s32[]{:S(2)}) async-start(), calls=%async_computation.5 | async-start | bytes 2359296 | tf_op jit(solution)/shard_map/all_gather | solution.py:124
  13.1 194.7 %all-gather.5.cloned.1.call-start = ((), (), s32[]{:S(2)}) async-start(), calls=%async_computation.2 | async-start | bytes 2359296 | tf_op jit(solution)/shard_map/all_gather | solution.py:85
  15.0 202.1 %all-gather.7.cloned.1.call-start = ((), (), s32[]{:S(2)}) async-start(), calls=%async_computation.3 | async-start | bytes 2359296 | tf_op jit(solution)/shard_map/all_gather | solution.py:86
  46.2 1.4 copy-start.2
  49.0 1.2 copy-start.7
  49.0 63.3 %copy-start.6 = (bf16[512,256]{0,1:T(8,128)(2,1)S(1)}, bf16[512,256]{0,1:T(8,128)(2,1)}, u32[]{:S(2)}) copy-start(bf16[512,256]{0,1:T(8,128)(2,1)} %convolution_convert_fusion) | copy-start | bytes 786436
  49.0 66.4 %copy-start.5 = (bf16[512,256]{0,1:T(8,128)(2,1)S(1)}, bf16[512,256]{0,1:T(8,128)(2,1)}, u32[]{:S(2)}) copy-start(bf16[512,256]{0,1:T(8,128)(2,1)} %copy.47) | copy-start | bytes 786436
  49.1 238.6 %reduce-scatter.2.cloned.1.call-start = ((), (), s32[]{:S(2)}) async-start(), calls=%async_computation.6 | async-start | bytes 2359296 | tf_op jit(solution)/shard_map/reduce_scatter | solution.py:182
  116.9 3.2 %copy-start.9 = (f32[2]{0:T(128)S(1)}, f32[2]{0:T(128)}, u32[]{:S(2)}) copy-start(f32[2]{0:T(128)} %get-tuple-element.847) | copy-start | bytes 28 | tf_op jit(solution)/shard_map/while/body/eval_jaxpr/cond
  123.1 2.3 copy-start.1
  127.6 3.2 %copy-start.9 = (f32[2]{0:T(128)S(1)}, f32[2]{0:T(128)}, u32[]{:S(2)}) copy-start(f32[2]{0:T(128)} %get-tuple-element.847) | copy-start | bytes 28 | tf_op jit(solution)/shard_map/while/body/eval_jaxpr/cond
  133.8 2.2 copy-start.1
  138.3 3.2 %copy-start.9 = (f32[2]{0:T(128)S(1)}, f32[2]{0:T(128)}, u32[]{:S(2)}) copy-start(f32[2]{0:T(128)} %get-tuple-element.847) | copy-start | bytes 28 | tf_op jit(solution)/shard_map/while/body/eval_jaxpr/cond
  144.5 2.3 copy-start.1
  149.0 3.2 %copy-start.9 = (f32[2]{0:T(128)S(1)}, f32[2]{0:T(128)}, u32[]{:S(2)}) copy-start(f32[2]{0:T(128)} %get-tuple-element.847) | copy-start | bytes 28 | tf_op jit(solution)/shard_map/while/body/eval_jaxpr/cond
  155.2 2.2 copy-start.1
  159.7 3.2 %copy-start.9 = (f32[2]{0:T(128)S(1)}, f32[2]{0:T(128)}, u32[]{:S(2)}) copy-start(f32[2]{0:T(128)} %get-tuple-element.847) | copy-start | bytes 28 | tf_op jit(solution)/shard_map/while/body/eval_jaxpr/cond
  165.9 2.2 copy-start.1
  170.3 3.2 %copy-start.9 = (f32[2]{0:T(128)S(1)}, f32[2]{0:T(128)}, u32[]{:S(2)}) copy-start(f32[2]{0:T(128)} %get-tuple-element.847) | copy-start | bytes 28 | tf_op jit(solution)/shard_map/while/body/eval_jaxpr/cond
  176.6 2.2 copy-start.1
  181.1 3.2 %copy-start.9 = (f32[2]{0:T(128)S(1)}, f32[2]{0:T(128)}, u32[]{:S(2)}) copy-start(f32[2]{0:T(128)} %get-tuple-element.847) | copy-start | bytes 28 | tf_op jit(solution)/shard_map/while/body/eval_jaxpr/cond
  187.3 2.2 copy-start.1
  191.7 3.2 %copy-start.9 = (f32[2]{0:T(128)S(1)}, f32[2]{0:T(128)}, u32[]{:S(2)}) copy-start(f32[2]{0:T(128)} %get-tuple-element.847) | copy-start | bytes 28 | tf_op jit(solution)/shard_map/while/body/eval_jaxpr/cond
  198.0 2.2 copy-start.1
  204.9 1.0 copy-start.3
  204.9 12.2 %copy-start.4 = (bf16[512,256]{0,1:T(8,128)(2,1)S(1)}, bf16[512,256]{0,1:T(8,128)(2,1)}, u32[]{:S(2)}) copy-start(bf16[512,256]{0,1:T(8,128)(2,1)} %copy.48) | copy-start | bytes 786436
  204.9 12.2 %copy-start.10 = (f32[2]{0:T(128)S(1)}, f32[2]{0:T(128)}, u32[]{:S(2)}) copy-start(f32[2]{0:T(128)} %get-tuple-element.1336) | copy-start | bytes 28
Sparse Core Ops, SparseCore 0:
  10.6 53.2 all-gather.8
  66.5 48.7 all-gather.10
  118.0 48.5 all-gather.4
  168.5 48.5 all-gather.6
  220.4 67.1 reduce-scatter.1
